TPU v7x, 32 devices: a whole 2x2x4 slice. The times are simulated.
32 devices in a mesh: ep: 8 (over z, y), tp: 4 (over x, core).
Axes of the slice: x: 2, y: 2, z: 4, core: 2. Of those that a mesh axis runs over, the one named last changes fastest.
Arguments:
- tokens: bfloat16 [128, 1024], P('ep'), may hold values from -6 to 6
- attn_gain: float32 [1024], replicated, may hold values from 0.1 to 1.9
- q_down: bfloat16 [1024, 512], P(None, 'tp'), may hold values from -0.1875 to 0.1875
- kv_down: bfloat16 [1024, 512], P(None, 'tp'), may hold values from -0.1875 to 0.1875
- rope_down: bfloat16 [1024, 32], replicated, may hold values from -0.1875 to 0.1875
- q_latent_gain: float32 [512], replicated, may hold values from 0.1 to 1.9
- kv_latent_gain: float32 [512], replicated, may hold values from 0.1 to 1.9
- q_up: bfloat16 [512, 768], P(None, 'tp'), may hold values from -0.25 to 0.25
- query_gain: float32 [8, 96], P('tp'), may hold values from 0.4 to 48
- key_up: bfloat16 [512, 512], P(None, 'tp'), may hold values from -0.25 to 0.25
- value_up: bfloat16 [512, 512], P(None, 'tp'), may hold values from -0.25 to 0.25
- attn_out: bfloat16 [512, 1024], P('tp'), may hold values from -0.25 to 0.25
- cache_latent: bfloat16 [128, 512, 512], P(('ep', 'tp')), may hold values from -6 to 6
- cache_rope: bfloat16 [128, 32, 512], P(('ep', 'tp')), may hold values from -6 to 6
- lengths: int32 [128], P('ep'), may hold values from 1 to 512, as said below
- moe_gain: float32 [1024], replicated, may hold values from 0.1 to 1.9
- route: int32 [128, 6], P('ep'), may hold values from 0 to 7, as said below
- route_weight: float32 [128, 6], P('ep'), may hold values from 0.1 to 1
- expert_gate: bfloat16 [8, 1024, 512], P('ep', None, 'tp'), may hold values from -0.1875 to 0.1875
- expert_up: bfloat16 [8, 1024, 512], P('ep', None, 'tp'), may hold values from -0.1875 to 0.1875
- expert_down: bfloat16 [8, 512, 1024], P('ep', 'tp'), may hold values from -0.25 to 0.25
Outputs:
- mixed_out: bfloat16 [128, 1024], P('ep', 'tp')
- new_latent: bfloat16 [128, 512], P('ep', 'tp')
- new_rope: bfloat16 [128, 32], P('ep')
Inputs may be any that keep to these rules, and one draw needn't show every extreme that they name: `route`: each row names 6 different experts that lie in one group of 8 consecutive expert numbers. Among the rows of the 16 sequences of one index of ep no expert is named more than 12 times, and some expert is named exactly 12 times by the rows of every index of ep. `lengths`: some sequence has exactly 512 cached positions.
All inputs are finite; a program needn't handle non-finite values.
Results may differ from a plain program's by a relative error of at most 0.02.
Values may be sent and summed in bfloat16 or wider, within the bound.
A program may use at most 64 MiB of HBM per device.

v0:
```python
import jax
import jax.numpy as jnp
from jax import lax
from jax.sharding import PartitionSpec as P

NOPE = 64
VDIM = 64
QK = 96
EPG = 8
EPS = 1e-06
ROPE_BASE = 10000.0


def rms_scaled(values_in, gain_vec):
    values_in = values_in.astype(jnp.float32)
    return (
        values_in
        * lax.rsqrt(jnp.mean(values_in * values_in, axis=-1, keepdims=True) + EPS)
        * gain_vec
    )


def rotate_last(values_in, positions):
    half_dim = values_in.shape[-1] // 2
    inverse = ROPE_BASE ** (-jnp.arange(half_dim, dtype=jnp.float32) / half_dim)
    angles = positions.astype(jnp.float32)[..., None] * inverse
    lower_half = values_in[..., :half_dim]
    upper_half = values_in[..., half_dim:]
    return jnp.concatenate(
        [
            lower_half * jnp.cos(angles) - upper_half * jnp.sin(angles),
            upper_half * jnp.cos(angles) + lower_half * jnp.sin(angles),
        ],
        -1,
    )


def rotate_rows(values_in, positions):
    half_dim = values_in.shape[1] // 2
    inverse = ROPE_BASE ** (-jnp.arange(half_dim, dtype=jnp.float32) / half_dim)
    angles = inverse[:, None] * positions.astype(jnp.float32)[None, :]
    lower_half = values_in[:, :half_dim]
    upper_half = values_in[:, half_dim:]
    return jnp.concatenate(
        [
            lower_half * jnp.cos(angles) - upper_half * jnp.sin(angles),
            upper_half * jnp.cos(angles) + lower_half * jnp.sin(angles),
        ],
        1,
    )


def shards(
    tokens,
    attn_gain,
    q_down,
    kv_down,
    rope_down,
    q_latent_gain,
    kv_latent_gain,
    q_up,
    query_gain,
    key_up,
    value_up,
    attn_out,
    cache_latent,
    cache_rope,
    lengths,
    moe_gain,
    route,
    route_weight,
    expert_gate,
    expert_up,
    expert_down,
):
    score_scale = QK ** (-0.5)
    tp_count = lax.axis_size("tp")
    tp_index = lax.axis_index("tp")
    normed = rms_scaled(tokens, attn_gain).astype(jnp.bfloat16)
    q_part = jnp.dot(normed, q_down, preferred_element_type=jnp.float32).astype(jnp.bfloat16)
    kv_part = jnp.dot(normed, kv_down, preferred_element_type=jnp.float32).astype(jnp.bfloat16)
    q_raw, kv_raw = (
        lax.all_gather(q_part, "tp", axis=1, tiled=True),
        lax.all_gather(kv_part, "tp", axis=1, tiled=True),
    )
    new_rope = jnp.dot(normed, rope_down, preferred_element_type=jnp.float32).astype(jnp.bfloat16)
    q_lat = rms_scaled(q_raw, q_latent_gain).astype(jnp.bfloat16)
    latent_new = rms_scaled(kv_raw, kv_latent_gain).astype(jnp.bfloat16)
    kv_cols = kv_part.shape[1]
    new_latent = lax.dynamic_slice_in_dim(latent_new, tp_index * kv_cols, kv_cols, 1)
    heads_here = query_gain.shape[0]
    seq_count = tokens.shape[0]
    query_head = rms_scaled(
        jnp.dot(q_lat, q_up, preferred_element_type=jnp.float32).reshape(seq_count, heads_here, QK),
        query_gain,
    )
    query_head = jnp.concatenate(
        [query_head[..., :NOPE], rotate_last(query_head[..., NOPE:], lengths[:, None])], -1
    ).astype(jnp.bfloat16)
    absorbed = jnp.einsum(
        "shn,rhn->shr",
        query_head[..., :NOPE],
        key_up.reshape(-1, heads_here, NOPE),
        preferred_element_type=jnp.float32,
    ).astype(jnp.bfloat16)
    rot_query = query_head[..., NOPE:]
    absorbed_mine, rot_mine = (
        lax.all_to_all(absorbed, "tp", split_axis=0, concat_axis=1, tiled=True),
        lax.all_to_all(rot_query, "tp", split_axis=0, concat_axis=1, tiled=True),
    )
    seqs_mine = cache_latent.shape[0]
    first_seq = tp_index * seqs_mine
    len_mine = lax.dynamic_slice_in_dim(lengths, first_seq, seqs_mine, 0)
    latent_mine = lax.dynamic_slice_in_dim(latent_new, first_seq, seqs_mine, 0)
    key_new = rotate_last(
        lax.dynamic_slice_in_dim(new_rope, first_seq, seqs_mine, 0).astype(jnp.float32), len_mine
    ).astype(jnp.bfloat16)
    positions = jnp.arange(cache_latent.shape[1], dtype=jnp.int32)
    rotated_keys = rotate_rows(cache_rope.astype(jnp.float32), positions).astype(jnp.bfloat16)
    scores = (
        jnp.einsum("shr,sjr->shj", absorbed_mine, cache_latent, preferred_element_type=jnp.float32)
        + jnp.einsum("shp,spj->shj", rot_mine, rotated_keys, preferred_element_type=jnp.float32)
    ) * score_scale
    self_score = (
        jnp.einsum("shr,sr->sh", absorbed_mine, latent_mine, preferred_element_type=jnp.float32)
        + jnp.einsum("shp,sp->sh", rot_mine, key_new, preferred_element_type=jnp.float32)
    ) * score_scale
    valid_keys = positions[None, :] < len_mine[:, None]
    masked = jnp.where(valid_keys[:, None, :], scores, -jnp.inf)
    row_max = jnp.maximum(jnp.max(masked, axis=-1), self_score)
    weights = jnp.exp(masked - row_max[..., None])
    self_weight = jnp.exp(self_score - row_max)
    total_weight = jnp.sum(weights, axis=-1) + self_weight
    latent_sum = jnp.einsum(
        "shj,sjr->shr",
        weights.astype(jnp.bfloat16),
        cache_latent,
        preferred_element_type=jnp.float32,
    )
    latent_sum = (
        latent_sum
        + self_weight.astype(jnp.bfloat16).astype(jnp.float32)[..., None]
        * latent_mine.astype(jnp.float32)[:, None, :]
    )
    attended = (latent_sum / total_weight[..., None]).astype(jnp.bfloat16)
    attended_heads = lax.all_to_all(attended, "tp", split_axis=1, concat_axis=0, tiled=True)
    head_values = (
        jnp.einsum(
            "shr,rhv->shv",
            attended_heads,
            value_up.reshape(-1, heads_here, VDIM),
            preferred_element_type=jnp.float32,
        )
        .astype(jnp.bfloat16)
        .reshape(seq_count, heads_here * VDIM)
    )
    head_sum = lax.psum(
        jnp.dot(head_values, attn_out, preferred_element_type=jnp.float32).astype(jnp.bfloat16),
        "tp",
    ).astype(jnp.float32)
    attn_resid = (tokens.astype(jnp.float32) + head_sum).astype(jnp.bfloat16)
    moe_input = rms_scaled(attn_resid, moe_gain).astype(jnp.bfloat16)
    topk_here = route.shape[1]
    experts_all = expert_gate.shape[0] * lax.axis_size("ep")
    group_cap = min(seq_count, max(2, 2 * seq_count * EPG // experts_all))
    capacity = (topk_here * group_cap + EPG - 1) // EPG
    flat_route = route.reshape(-1)
    row_order = jnp.arange(flat_route.shape[0])
    slot_rank = jnp.sum(
        (flat_route[:, None] == flat_route[None, :]) & (row_order[None, :] < row_order[:, None]),
        axis=1,
    )
    slot_index = flat_route * capacity + slot_rank
    model_width = tokens.shape[1]
    quarter_cols = model_width // tp_count
    residual = lax.dynamic_slice_in_dim(attn_resid, tp_index * quarter_cols, quarter_cols, 1)
    own_cols = lax.dynamic_slice_in_dim(moe_input, tp_index * quarter_cols, quarter_cols, 1)
    buffer = jnp.zeros((experts_all * capacity, own_cols.shape[1]), jnp.bfloat16)
    buffer = buffer.at[slot_index].set(jnp.repeat(own_cols, topk_here, axis=0))
    arrived = lax.all_to_all(
        buffer.reshape(experts_all, capacity, own_cols.shape[1]),
        "ep",
        split_axis=0,
        concat_axis=1,
        tiled=True,
    )
    piece = lax.all_gather(arrived, "tp", axis=2, tiled=True)
    gate_pre = jnp.einsum("erd,edf->erf", piece, expert_gate, preferred_element_type=jnp.float32)
    up_pre = jnp.einsum("erd,edf->erf", piece, expert_up, preferred_element_type=jnp.float32)
    hidden = (jax.nn.silu(gate_pre) * up_pre).astype(jnp.bfloat16)
    partial_value = jnp.einsum(
        "erf,efd->erd", hidden, expert_down, preferred_element_type=jnp.float32
    )
    reduced = lax.psum_scatter(
        partial_value.astype(jnp.bfloat16), "tp", scatter_dimension=2, tiled=True
    )
    returned = lax.all_to_all(reduced, "ep", split_axis=1, concat_axis=0, tiled=True)
    picked = (
        returned.reshape(-1, quarter_cols)[slot_index]
        .astype(jnp.float32)
        .reshape(seq_count, topk_here, quarter_cols)
    )
    mixed_out = (
        residual.astype(jnp.float32) + jnp.sum(picked * route_weight[..., None], axis=1)
    ).astype(jnp.bfloat16)
    return (mixed_out, new_latent, new_rope)


def solution(mesh):
    placed = (
        P("ep", None),
        P(),
        P(None, "tp"),
        P(None, "tp"),
        P(),
        P(),
        P(),
        P(None, "tp"),
        P("tp", None),
        P(None, "tp"),
        P(None, "tp"),
        P("tp", None),
        P(("ep", "tp"), None, None),
        P(("ep", "tp"), None, None),
        P("ep"),
        P(),
        P("ep", None),
        P("ep", None),
        P("ep", None, "tp"),
        P("ep", None, "tp"),
        P("ep", "tp", None),
    )
    return jax.shard_map(
        shards,
        mesh=mesh,
        in_specs=placed,
        out_specs=(P("ep", "tp"), P("ep", "tp"), P("ep", None)),
        check_vma=False,
    )
```

profile of v0, /device:TPU:0, one launch (start us, length us, event | category | flops | bytes accessed | tf_op | source)
XLA Modules:
  0.0 125.3 jit_solution(8537989430489213607)
XLA Ops:
  7.2 1.0 fusion.19
  8.3 1.2 convolution_convert_fusion.6
  9.5 6.1 %all_gather.9 = bf16[16,512]{1,0:T(8,128)(2,1)S(1)} all-gather(bf16[16,128]{1,0:T(8,128)(2,1)S(1)} %convolution_convert_fusion.6), channel_id=1, replica_groups=mesh['ep'=8,'tp'=4] {'tp'}, dimensions={1}, use_global_device_ids=true | all-gather | bytes 20480 | tf_op jit(solution)/shard_map/all_gather | solution.py:83
  15.7 1.1 fusion.42
  19.5 3.3 %all-to-all-start.1 = ((bf16[4,2,128]{2,1,0:T(2,128)(2,1)}), bf16[4,2,128]{2,1,0:T(2,128)(2,1)S(1)}, u32[]{:S(2)}, u32[]{:S(2)}) async-start(bf16[4,2,128]{2,1,0:T(2,128)(2,1)} %reshape.330), calls=%async_computation.1 | async-start | bytes 4096 | tf_op jit(solution)/shard_map/all_to_all | solution.py:109
  24.5 1.0 copy.90
  25.7 0.9 convert_element_type.133
  27.6 1.2 convolution_convert_fusion.5
  28.8 5.4 %all_gather.10 = bf16[16,512]{1,0:T(8,128)(2,1)S(1)} all-gather(bf16[16,128]{1,0:T(8,128)(2,1)S(1)} %convolution_convert_fusion.5), channel_id=1, replica_groups=mesh['ep'=8,'tp'=4] {'tp'}, dimensions={1}, use_global_device_ids=true | all-gather | bytes 20480 | tf_op jit(solution)/shard_map/all_gather | solution.py:84
  35.7 3.3 %all-to-all-start = ((bf16[16,2,512]{2,1,0:T(2,128)(2,1)}), bf16[16,2,512]{2,1,0:T(2,128)(2,1)S(1)}, u32[]{:S(2)}, u32[]{:S(2)}) async-start(bf16[16,2,512]{2,1,0:T(2,128)(2,1)} %copy.91), calls=%async_computation | async-start | bytes 65536 | tf_op jit(solution)/shard_map/all_to_all | solution.py:108
  39.2 3.7 %all-to-all-done = bf16[16,2,512]{2,1,0:T(2,128)(2,1)S(1)} async-done(((bf16[16,2,512]{2,1,0:T(2,128)(2,1)}), bf16[16,2,512]{2,1,0:T(2,128)(2,1)S(1)}, u32[]{:S(2)}, u32[]{:S(2)}) %all-to-all-start) | async-done | bytes 32800 | tf_op jit(solution)/shard_map/all_to_all | solution.py:108
  45.3 3.3 %all-to-all-start.2 = ((bf16[4,8,512]{2,0,1:T(4,128)(2,1)}), bf16[4,8,512]{2,0,1:T(4,128)(2,1)S(1)}, u32[]{:S(2)}, u32[]{:S(2)}) async-start(bf16[4,8,512]{2,0,1:T(4,128)(2,1)} %copy.95), calls=%async_computation.2 | async-start | bytes 65536 | tf_op jit(solution)/shard_map/all_to_all | solution.py:146
  49.5 2.9 %all-to-all-done.2 = bf16[4,8,512]{2,0,1:T(4,128)(2,1)S(1)} async-done(((bf16[4,8,512]{2,0,1:T(4,128)(2,1)}), bf16[4,8,512]{2,0,1:T(4,128)(2,1)S(1)}, u32[]{:S(2)}, u32[]{:S(2)}) %all-to-all-start.2) | async-done | bytes 32800 | tf_op jit(solution)/shard_map/all_to_all | solution.py:146
  52.9 10.3 %psum.7 = bf16[16,1024]{1,0:T(8,128)(2,1)S(1)} all-reduce(bf16[16,1024]{1,0:T(8,128)(2,1)S(1)} %convolution_convert_fusion.1), channel_id=1, replica_groups=mesh['ep'=8,'tp'=4] {'tp'}, use_global_device_ids=true, to_apply=%region_6.7 | all-reduce | flops 16384 | bytes 65536 | tf_op jit(solution)/shard_map/psum | solution.py:157
  63.4 0.9 scatter_custom_fusion
  64.4 12.8 %all_to_all.75 = bf16[8,12,256]{2,1,0:T(8,128)(2,1)S(1)} all-to-all(bf16[8,12,256]{2,1,0:T(8,128)(2,1)S(1)} %reshape.301), channel_id=1, replica_groups=mesh['ep'=8,'tp'=4] {'ep'}, dimensions={0} | all-to-all | bytes 98304 | tf_op jit(solution)/shard_map/all_to_all | solution.py:180
  77.2 5.6 %all_gather.11 = bf16[1,96,1024]{2,1,0:T(8,128)(2,1)S(1)} all-gather(bf16[1,96,256]{2,1,0:T(8,128)(2,1)S(1)} %all_to_all.68), channel_id=1, replica_groups=mesh['ep'=8,'tp'=4] {'tp'}, dimensions={2}, use_global_device_ids=true | all-gather | bytes 245760 | tf_op jit(solution)/shard_map/all_gather | solution.py:187
  83.1 1.0 fusion
  84.2 17.4 %reduce-scatter.2.cloned.1.call-done = bf16[1,96,256]{2,1,0:T(8,128)(2,1)} async-done(((bf16[1,96,1024]{2,1,0:T(8,128)(2,1)}), bf16[1,96,256]{2,1,0:T(8,128)(2,1)}) %reduce-scatter.2.cloned.1.call-update) | async-done | bytes 49168 | tf_op jit(solution)/shard_map/reduce_scatter | solution.py:194
  101.6 0.9 copy.122
  103.0 0.9 reduce
  104.6 5.5 %all-to-all-start.4 = ((bf16[8,2,1536]{2,1,0:T(2,128)(2,1)}), bf16[8,2,1536]{2,1,0:T(2,128)(2,1)S(1)}, u32[]{:S(2)}, u32[]{:S(2)}) async-start(bf16[8,2,1536]{2,1,0:T(2,128)(2,1)} %reshape.332), calls=%async_computation.5 | async-start | bytes 98304 | tf_op jit(solution)/shard_map/all_to_all | solution.py:197
  110.7 6.2 %all-to-all-done.4 = bf16[8,2,1536]{2,1,0:T(2,128)(2,1)S(1)} async-done(((bf16[8,2,1536]{2,1,0:T(2,128)(2,1)}), bf16[8,2,1536]{2,1,0:T(2,128)(2,1)S(1)}, u32[]{:S(2)}, u32[]{:S(2)}) %all-to-all-start.4) | async-done | bytes 49184 | tf_op jit(solution)/shard_map/all_to_all | solution.py:197
  116.9 0.8 gather_fusion
  (104 shorter events, 14.1 us)
Async XLA Ops:
  7.2 35.8 %copy-start = (bf16[4,512,512]{2,1,0:T(8,128)(2,1)S(1)}, bf16[4,512,512]{2,1,0:T(8,128)(2,1)}, u32[]{:S(2)}) copy-start(bf16[4,512,512]{2,1,0:T(8,128)(2,1)} %param.33) | copy-start | bytes 6291460
  7.2 27.3 %copy-start.5 = (bf16[16,1024]{1,0:T(8,128)(2,1)S(1)}, bf16[16,1024]{1,0:T(8,128)(2,1)}, u32[]{:S(2)}) copy-start(bf16[16,1024]{1,0:T(8,128)(2,1)} %param.21) | copy-start | bytes 98308
  7.2 27.3 %copy-start.11 = (f32[1024]{0:T(1024)S(1)}, f32[1024]{0:T(1024)}, u32[]{:S(2)}) copy-start(f32[1024]{0:T(1024)} %param.22) | copy-start | bytes 12292
  7.2 27.1 %copy-start.8 = (f32[512]{0:T(512)S(1)}, f32[512]{0:T(512)}, u32[]{:S(2)}) copy-start(f32[512]{0:T(512)} %param.27) | copy-start | bytes 6148
  7.2 27.2 %copy-start.10 = (bf16[1024,32]{0,1:T(8,128)(2,1)S(1)}, bf16[1024,32]{0,1:T(8,128)(2,1)}, u32[]{:S(2)}) copy-start(bf16[1024,32]{0,1:T(8,128)(2,1)} %param.25) | copy-start | bytes 196612
  19.5 16.2 %all-to-all-start.1 = ((bf16[4,2,128]{2,1,0:T(2,128)(2,1)}), bf16[4,2,128]{2,1,0:T(2,128)(2,1)S(1)}, u32[]{:S(2)}, u32[]{:S(2)}) async-start(bf16[4,2,128]{2,1,0:T(2,128)(2,1)} %reshape.330), calls=%async_computation.1 | async-start | bytes 4096 | tf_op jit(solution)/shard_map/all_to_all | solution.py:109
  34.7 10.0 %copy-start.9 = (bf16[16,32]{1,0:T(8,128)(2,1)}, bf16[16,32]{1,0:T(8,128)(2,1)S(1)}, u32[]{:S(2)}) copy-start(bf16[16,32]{1,0:T(8,128)(2,1)S(1)} %convolution_convert_fusion.4) | copy-start | bytes 3076
  35.7 7.2 %all-to-all-start = ((bf16[16,2,512]{2,1,0:T(2,128)(2,1)}), bf16[16,2,512]{2,1,0:T(2,128)(2,1)S(1)}, u32[]{:S(2)}, u32[]{:S(2)}) async-start(bf16[16,2,512]{2,1,0:T(2,128)(2,1)} %copy.91), calls=%async_computation | async-start | bytes 65536 | tf_op jit(solution)/shard_map/all_to_all | solution.py:108
  43.0 5.6 %copy-start.6 = (bf16[512,128]{1,0:T(8,128)(2,1)S(1)}, bf16[512,128]{1,0:T(8,128)(2,1)}, u32[]{:S(2)}) copy-start(bf16[512,128]{1,0:T(8,128)(2,1)} %param.31) | copy-start | bytes 393220
  43.6 9.1 %copy-start.1 = (bf16[128,1024]{1,0:T(8,128)(2,1)S(1)}, bf16[128,1024]{1,0:T(8,128)(2,1)}, u32[]{:S(2)}) copy-start(bf16[128,1024]{1,0:T(8,128)(2,1)} %param.32) | copy-start | bytes 786436
  44.2 38.6 %copy-start.2 = (bf16[1,1024,128]{2,1,0:T(8,128)(2,1)S(1)}, bf16[1,1024,128]{2,1,0:T(8,128)(2,1)}, u32[]{:S(2)}) copy-start(bf16[1,1024,128]{2,1,0:T(8,128)(2,1)} %param.39) | copy-start | bytes 786436
  44.2 38.8 %copy-start.3 = (bf16[1,128,1024]{2,1,0:T(8,128)(2,1)S(1)}, bf16[1,128,1024]{2,1,0:T(8,128)(2,1)}, u32[]{:S(2)}) copy-start(bf16[1,128,1024]{2,1,0:T(8,128)(2,1)} %param.41) | copy-start | bytes 786436
  44.2 38.8 %copy-start.4 = (bf16[1,1024,128]{2,1,0:T(8,128)(2,1)S(1)}, bf16[1,1024,128]{2,1,0:T(8,128)(2,1)}, u32[]{:S(2)}) copy-start(bf16[1,1024,128]{2,1,0:T(8,128)(2,1)} %param.40) | copy-start | bytes 786436
  44.7 39.5 %copy-start.7 = (f32[16,6]{0,1:T(8,128)S(1)}, f32[16,6]{0,1:T(8,128)}, u32[]{:S(2)}) copy-start(f32[16,6]{0,1:T(8,128)} %param.38) | copy-start | bytes 1156
  45.3 7.2 %all-to-all-start.2 = ((bf16[4,8,512]{2,0,1:T(4,128)(2,1)}), bf16[4,8,512]{2,0,1:T(4,128)(2,1)S(1)}, u32[]{:S(2)}, u32[]{:S(2)}) async-start(bf16[4,8,512]{2,0,1:T(4,128)(2,1)} %copy.95), calls=%async_computation.2 | async-start | bytes 65536 | tf_op jit(solution)/shard_map/all_to_all | solution.py:146
  48.6 53.1 %reduce-scatter.2.cloned.1.call-start = ((), (), s32[]{:S(2)}) async-start(), calls=%async_computation.6 | async-start | bytes 245760 | tf_op jit(solution)/shard_map/reduce_scatter | solution.py:194
  104.6 12.3 %all-to-all-start.4 = ((bf16[8,2,1536]{2,1,0:T(2,128)(2,1)}), bf16[8,2,1536]{2,1,0:T(2,128)(2,1)S(1)}, u32[]{:S(2)}, u32[]{:S(2)}) async-start(bf16[8,2,1536]{2,1,0:T(2,128)(2,1)} %reshape.332), calls=%async_computation.5 | async-start | bytes 98304 | tf_op jit(solution)/shard_map/all_to_all | solution.py:197
Sparse Core Ops, SparseCore 0:
  84.2 17.3 reduce-scatter.1
where the time goes:
time: 126 us; the launch traced here: 125 us
  blocking collectives  40.2 us (32%)
  waiting for transfers between devices  30.3 us (24%)
  starting transfers between devices  15.3 us (12%)
  between operations  14.4 us (11%)
  local copies, waits for them, and re-layouts  9.87 us (8%)
  other arithmetic  8.27 us (7%)
  matrix products  6.88 us (5%)
    reduce_scatter x1, waiting for transfers between devices, shards(): lax.psum_scatter(partial_value.astype(jnp.bfloat16), 'tp', scatter_dimens...  17.4 us
    all_to_all x1, blocking collectives, shards(): lax.all_to_all(buffer.reshape(experts_all, capacity, own_cols.shape[1]),...  12.8 us
    psum x1, blocking collectives, shards(): lax.psum(jnp.dot(head_values, attn_out, preferred_element_type=jnp.float3...  10.3 us
    all_to_all x1, waiting for transfers between devices, shards(): lax.all_to_all(reduced, 'ep', split_axis=1, concat_axis=0, tiled=True)  6.2 us
    all_gather x1, blocking collectives, shards(): lax.all_gather(q_part, 'tp', axis=1, tiled=True)  6.14 us
    all_gather x1, blocking collectives, shards(): piece = lax.all_gather(arrived, 'tp', axis=2, tiled=True)  5.6 us
    all_to_all x1, starting transfers between devices, shards(): lax.all_to_all(reduced, 'ep', split_axis=1, concat_axis=0, tiled=True)  5.52 us
    all_gather x1, blocking collectives, shards(): lax.all_gather(kv_part, 'tp', axis=1, tiled=True)  5.42 us
  transfers between devices with their start and end apart: 5, of which 4 were waited for; matrix products, arithmetic and copies ran while one was open for 7% of the time, Pallas kernels for 0%

commit v1 on v0

--- a/solution.py
+++ b/solution.py
@@ -73,6 +73,10 @@
     expert_up,
     expert_down,
 ):
+
+    def hold_the_slabs(t0, along_axis):
+        return lax.all_gather(t0, along_axis).sum(axis=0)
+
     score_scale = QK ** (-0.5)
     tp_count = lax.axis_size("tp")
     tp_index = lax.axis_index("tp")
@@ -154,9 +158,9 @@
         .astype(jnp.bfloat16)
         .reshape(seq_count, heads_here * VDIM)
     )
-    head_sum = lax.psum(
+    head_sum = hold_the_slabs(
         jnp.dot(head_values, attn_out, preferred_element_type=jnp.float32).astype(jnp.bfloat16),
-        "tp",
+        along_axis="tp",
     ).astype(jnp.float32)
     attn_resid = (tokens.astype(jnp.float32) + head_sum).astype(jnp.bfloat16)
     moe_input = rms_scaled(attn_resid, moe_gain).astype(jnp.bfloat16)

time: 126 us -> 120 us (0.952)
  blocking collectives: 40.2 us -> 35.4 us
    psum x1 -> x0, blocking collectives: 10.3 us -> none  [shards(): lax.psum(jnp.dot(head_values, attn_out, preferred_element_type=jnp.float3...]
    all_gather x0 -> x1, blocking collectives: none -> 5.41 us  [hold_the_slabs(): return lax.all_gather(t0, along_axis).sum(axis=0)]
  transfers between devices with their start and end apart: 5 -> 5, of which waited for: 4 -> 4; matrix products, arithmetic and copies ran while one was open for 7% -> 8% of each run, Pallas kernels for 0% -> 0%
where the time goes in v1:
time: 120 us; the launch traced here: 119 us
  blocking collectives  35.4 us (30%)
  waiting for transfers between devices  29.3 us (24%)
  starting transfers between devices  15.3 us (13%)
  between operations  14.4 us (12%)
  local copies, waits for them, and re-layouts  9.87 us (8%)
  other arithmetic  8.29 us (7%)
  matrix products  6.87 us (6%)
    reduce_scatter x1, waiting for transfers between devices, shards(): lax.psum_scatter(partial_value.astype(jnp.bfloat16), 'tp', scatter_dimens...  16.4 us
    all_to_all x1, blocking collectives, shards(): lax.all_to_all(buffer.reshape(experts_all, capacity, own_cols.shape[1]),...  12.8 us
    all_to_all x1, waiting for transfers between devices, shards(): lax.all_to_all(reduced, 'ep', split_axis=1, concat_axis=0, tiled=True)  6.2 us
    all_gather x1, blocking collectives, shards(): lax.all_gather(q_part, 'tp', axis=1, tiled=True)  6.14 us
    all_gather x1, blocking collectives, shards(): piece = lax.all_gather(arrived, 'tp', axis=2, tiled=True)  5.6 us
    all_to_all x1, starting transfers between devices, shards(): lax.all_to_all(reduced, 'ep', split_axis=1, concat_axis=0, tiled=True)  5.52 us
    all_gather x1, blocking collectives, shards(): lax.all_gather(kv_part, 'tp', axis=1, tiled=True)  5.42 us
    all_gather x1, blocking collectives, hold_the_slabs(): return lax.all_gather(t0, along_axis).sum(axis=0)  5.41 us
  transfers between devices with their start and end apart: 5, of which 4 were waited for; matrix products, arithmetic and copies ran while one was open for 8% of the time, Pallas kernels for 0%

profile of v1, /device:TPU:0, one launch (start us, length us, event | category | flops | bytes accessed | tf_op | source)
XLA Modules:
  0.0 119.5 jit_solution(2239073504966215824)
XLA Ops:
  7.2 1.0 fusion.19
  8.3 1.2 convolution_convert_fusion.6
  9.5 6.1 %all_gather.15 = bf16[16,512]{1,0:T(8,128)(2,1)S(1)} all-gather(bf16[16,128]{1,0:T(8,128)(2,1)S(1)} %convolution_convert_fusion.6), channel_id=1, replica_groups=mesh['ep'=8,'tp'=4] {'tp'}, dimensions={1}, use_global_device_ids=true | all-gather | bytes 20480 | tf_op jit(solution)/shard_map/all_gather | solution.py:87
  15.7 1.1 fusion.42
  19.5 3.3 %all-to-all-start.1 = ((bf16[4,2,128]{2,1,0:T(2,128)(2,1)}), bf16[4,2,128]{2,1,0:T(2,128)(2,1)S(1)}, u32[]{:S(2)}, u32[]{:S(2)}) async-start(bf16[4,2,128]{2,1,0:T(2,128)(2,1)} %reshape.331), calls=%async_computation.1 | async-start | bytes 4096 | tf_op jit(solution)/shard_map/all_to_all | solution.py:113
  24.5 1.0 copy.90
  25.7 0.9 convert_element_type.135
  27.6 1.2 convolution_convert_fusion.5
  28.8 5.4 %all_gather.16 = bf16[16,512]{1,0:T(8,128)(2,1)S(1)} all-gather(bf16[16,128]{1,0:T(8,128)(2,1)S(1)} %convolution_convert_fusion.5), channel_id=1, replica_groups=mesh['ep'=8,'tp'=4] {'tp'}, dimensions={1}, use_global_device_ids=true | all-gather | bytes 20480 | tf_op jit(solution)/shard_map/all_gather | solution.py:88
  35.7 3.3 %all-to-all-start = ((bf16[16,2,512]{2,1,0:T(2,128)(2,1)}), bf16[16,2,512]{2,1,0:T(2,128)(2,1)S(1)}, u32[]{:S(2)}, u32[]{:S(2)}) async-start(bf16[16,2,512]{2,1,0:T(2,128)(2,1)} %copy.91), calls=%async_computation | async-start | bytes 65536 | tf_op jit(solution)/shard_map/all_to_all | solution.py:112
  39.2 3.7 %all-to-all-done = bf16[16,2,512]{2,1,0:T(2,128)(2,1)S(1)} async-done(((bf16[16,2,512]{2,1,0:T(2,128)(2,1)}), bf16[16,2,512]{2,1,0:T(2,128)(2,1)S(1)}, u32[]{:S(2)}, u32[]{:S(2)}) %all-to-all-start) | async-done | bytes 32800 | tf_op jit(solution)/shard_map/all_to_all | solution.py:112
  45.3 3.3 %all-to-all-start.2 = ((bf16[4,8,512]{2,0,1:T(4,128)(2,1)}), bf16[4,8,512]{2,0,1:T(4,128)(2,1)S(1)}, u32[]{:S(2)}, u32[]{:S(2)}) async-start(bf16[4,8,512]{2,0,1:T(4,128)(2,1)} %copy.95), calls=%async_computation.2 | async-start | bytes 65536 | tf_op jit(solution)/shard_map/all_to_all | solution.py:150
  49.5 2.9 %all-to-all-done.2 = bf16[4,8,512]{2,0,1:T(4,128)(2,1)S(1)} async-done(((bf16[4,8,512]{2,0,1:T(4,128)(2,1)}), bf16[4,8,512]{2,0,1:T(4,128)(2,1)S(1)}, u32[]{:S(2)}, u32[]{:S(2)}) %all-to-all-start.2) | async-done | bytes 32800 | tf_op jit(solution)/shard_map/all_to_all | solution.py:150
  52.9 5.4 %all-gather = bf16[64,1024]{1,0:T(8,128)(2,1)S(1)} all-gather(bf16[16,1024]{1,0:T(8,128)(2,1)S(1)} %convolution_convert_fusion.1), channel_id=2, replica_groups=mesh['ep'=8,'tp'=4] {'tp'}, dimensions={0}, use_global_device_ids=true | all-gather | bytes 163840 | tf_op jit(solution)/shard_map/all_gather | solution.py:78
  58.6 0.9 scatter_custom_fusion
  59.6 12.8 %all_to_all.75 = bf16[8,12,256]{2,1,0:T(8,128)(2,1)S(1)} all-to-all(bf16[8,12,256]{2,1,0:T(8,128)(2,1)S(1)} %reshape.301), channel_id=1, replica_groups=mesh['ep'=8,'tp'=4] {'ep'}, dimensions={0} | all-to-all | bytes 98304 | tf_op jit(solution)/shard_map/all_to_all | solution.py:184
  72.4 5.6 %all_gather.19 = bf16[1,96,1024]{2,1,0:T(8,128)(2,1)S(1)} all-gather(bf16[1,96,256]{2,1,0:T(8,128)(2,1)S(1)} %all_to_all.68), channel_id=1, replica_groups=mesh['ep'=8,'tp'=4] {'tp'}, dimensions={2}, use_global_device_ids=true | all-gather | bytes 245760 | tf_op jit(solution)/shard_map/all_gather | solution.py:191
  78.2 1.0 fusion
  79.4 16.4 %reduce-scatter.2.cloned.1.call-done = bf16[1,96,256]{2,1,0:T(8,128)(2,1)} async-done(((bf16[1,96,1024]{2,1,0:T(8,128)(2,1)}), bf16[1,96,256]{2,1,0:T(8,128)(2,1)}) %reduce-scatter.2.cloned.1.call-update) | async-done | bytes 49168 | tf_op jit(solution)/shard_map/reduce_scatter | solution.py:198
  95.8 0.9 copy.122
  97.2 0.9 reduce.1
  98.7 5.5 %all-to-all-start.4 = ((bf16[8,2,1536]{2,1,0:T(2,128)(2,1)}), bf16[8,2,1536]{2,1,0:T(2,128)(2,1)S(1)}, u32[]{:S(2)}, u32[]{:S(2)}) async-start(bf16[8,2,1536]{2,1,0:T(2,128)(2,1)} %reshape.333), calls=%async_computation.5 | async-start | bytes 98304 | tf_op jit(solution)/shard_map/all_to_all | solution.py:201
  104.9 6.2 %all-to-all-done.4 = bf16[8,2,1536]{2,1,0:T(2,128)(2,1)S(1)} async-done(((bf16[8,2,1536]{2,1,0:T(2,128)(2,1)}), bf16[8,2,1536]{2,1,0:T(2,128)(2,1)S(1)}, u32[]{:S(2)}, u32[]{:S(2)}) %all-to-all-start.4) | async-done | bytes 49184 | tf_op jit(solution)/shard_map/all_to_all | solution.py:201
  111.1 0.8 gather_fusion
  (105 shorter events, 14.1 us)
Async XLA Ops:
  7.2 35.8 %copy-start = (bf16[4,512,512]{2,1,0:T(8,128)(2,1)S(1)}, bf16[4,512,512]{2,1,0:T(8,128)(2,1)}, u32[]{:S(2)}) copy-start(bf16[4,512,512]{2,1,0:T(8,128)(2,1)} %param.33) | copy-start | bytes 6291460
  7.2 27.3 %copy-start.5 = (bf16[16,1024]{1,0:T(8,128)(2,1)S(1)}, bf16[16,1024]{1,0:T(8,128)(2,1)}, u32[]{:S(2)}) copy-start(bf16[16,1024]{1,0:T(8,128)(2,1)} %param.21) | copy-start | bytes 98308
  7.2 27.3 %copy-start.11 = (f32[1024]{0:T(1024)S(1)}, f32[1024]{0:T(1024)}, u32[]{:S(2)}) copy-start(f32[1024]{0:T(1024)} %param.22) | copy-start | bytes 12292
  7.2 27.1 %copy-start.8 = (f32[512]{0:T(512)S(1)}, f32[512]{0:T(512)}, u32[]{:S(2)}) copy-start(f32[512]{0:T(512)} %param.27) | copy-start | bytes 6148
  7.2 27.2 %copy-start.10 = (bf16[1024,32]{0,1:T(8,128)(2,1)S(1)}, bf16[1024,32]{0,1:T(8,128)(2,1)}, u32[]{:S(2)}) copy-start(bf16[1024,32]{0,1:T(8,128)(2,1)} %param.25) | copy-start | bytes 196612
  19.5 16.2 %all-to-all-start.1 = ((bf16[4,2,128]{2,1,0:T(2,128)(2,1)}), bf16[4,2,128]{2,1,0:T(2,128)(2,1)S(1)}, u32[]{:S(2)}, u32[]{:S(2)}) async-start(bf16[4,2,128]{2,1,0:T(2,128)(2,1)} %reshape.331), calls=%async_computation.1 | async-start | bytes 4096 | tf_op jit(solution)/shard_map/all_to_all | solution.py:113
  34.7 10.0 %copy-start.9 = (bf16[16,32]{1,0:T(8,128)(2,1)}, bf16[16,32]{1,0:T(8,128)(2,1)S(1)}, u32[]{:S(2)}) copy-start(bf16[16,32]{1,0:T(8,128)(2,1)S(1)} %convolution_convert_fusion.4) | copy-start | bytes 3076
  35.7 7.2 %all-to-all-start = ((bf16[16,2,512]{2,1,0:T(2,128)(2,1)}), bf16[16,2,512]{2,1,0:T(2,128)(2,1)S(1)}, u32[]{:S(2)}, u32[]{:S(2)}) async-start(bf16[16,2,512]{2,1,0:T(2,128)(2,1)} %copy.91), calls=%async_computation | async-start | bytes 65536 | tf_op jit(solution)/shard_map/all_to_all | solution.py:112
  43.0 5.6 %copy-start.6 = (bf16[512,128]{1,0:T(8,128)(2,1)S(1)}, bf16[512,128]{1,0:T(8,128)(2,1)}, u32[]{:S(2)}) copy-start(bf16[512,128]{1,0:T(8,128)(2,1)} %param.31) | copy-start | bytes 393220
  43.6 9.1 %copy-start.1 = (bf16[128,1024]{1,0:T(8,128)(2,1)S(1)}, bf16[128,1024]{1,0:T(8,128)(2,1)}, u32[]{:S(2)}) copy-start(bf16[128,1024]{1,0:T(8,128)(2,1)} %param.32) | copy-start | bytes 786436
  44.2 33.8 %copy-start.2 = (bf16[1,1024,128]{2,1,0:T(8,128)(2,1)S(1)}, bf16[1,1024,128]{2,1,0:T(8,128)(2,1)}, u32[]{:S(2)}) copy-start(bf16[1,1024,128]{2,1,0:T(8,128)(2,1)} %param.39) | copy-start | bytes 786436
  44.2 34.0 %copy-start.3 = (bf16[1,128,1024]{2,1,0:T(8,128)(2,1)S(1)}, bf16[1,128,1024]{2,1,0:T(8,128)(2,1)}, u32[]{:S(2)}) copy-start(bf16[1,128,1024]{2,1,0:T(8,128)(2,1)} %param.41) | copy-start | bytes 786436
  44.2 34.0 %copy-start.4 = (bf16[1,1024,128]{2,1,0:T(8,128)(2,1)S(1)}, bf16[1,1024,128]{2,1,0:T(8,128)(2,1)}, u32[]{:S(2)}) copy-start(bf16[1,1024,128]{2,1,0:T(8,128)(2,1)} %param.40) | copy-start | bytes 786436
  44.7 34.6 %copy-start.7 = (f32[16,6]{0,1:T(8,128)S(1)}, f32[16,6]{0,1:T(8,128)}, u32[]{:S(2)}) copy-start(f32[16,6]{0,1:T(8,128)} %param.38) | copy-start | bytes 1156
  45.3 7.2 %all-to-all-start.2 = ((bf16[4,8,512]{2,0,1:T(4,128)(2,1)}), bf16[4,8,512]{2,0,1:T(4,128)(2,1)S(1)}, u32[]{:S(2)}, u32[]{:S(2)}) async-start(bf16[4,8,512]{2,0,1:T(4,128)(2,1)} %copy.95), calls=%async_computation.2 | async-start | bytes 65536 | tf_op jit(solution)/shard_map/all_to_all | solution.py:150
  48.6 47.2 %reduce-scatter.2.cloned.1.call-start = ((), (), s32[]{:S(2)}) async-start(), calls=%async_computation.6 | async-start | bytes 245760 | tf_op jit(solution)/shard_map/reduce_scatter | solution.py:198
  98.7 12.3 %all-to-all-start.4 = ((bf16[8,2,1536]{2,1,0:T(2,128)(2,1)}), bf16[8,2,1536]{2,1,0:T(2,128)(2,1)S(1)}, u32[]{:S(2)}, u32[]{:S(2)}) async-start(bf16[8,2,1536]{2,1,0:T(2,128)(2,1)} %reshape.333), calls=%async_computation.5 | async-start | bytes 98304 | tf_op jit(solution)/shard_map/all_to_all | solution.py:201
Sparse Core Ops, SparseCore 0:
  79.4 16.3 reduce-scatter.1
